TPU v7x, 32 devices: a whole 2x2x4 slice. The times are simulated.
32 devices in a mesh: grp: 1, fs: 2 (over x), tp: 16 (over z, y, core).
Axes of the slice: x: 2, y: 2, z: 4, core: 2. Of those that a mesh axis runs over, the one named last changes fastest.
Arguments:
- prompt_rows: bfloat16 [512, 2048], P(('grp', 'fs')), may hold values from -6 to 6
- gain_before: float32 [2048], P('fs'), may hold values from 0.1 to 1.9
- gate_before: float32 [2048, 5632], P('fs', 'tp'), may hold values from -0.125 to 0.125
- up_before: float32 [2048, 5632], P('fs', 'tp'), may hold values from -0.125 to 0.125
- down_before: float32 [5632, 2048], P('fs', 'tp'), may hold values from -0.3125 to 0.3125
- gain_after: float32 [2048], P('fs'), may hold values from 0.1 to 1.9
- gate_after: float32 [2048, 5632], P('fs', 'tp'), may hold values from -0.125 to 0.125
- up_after: float32 [2048, 5632], P('fs', 'tp'), may hold values from -0.125 to 0.125
- down_after: float32 [5632, 2048], P('fs', 'tp'), may hold values from -0.3125 to 0.3125
Outputs:
- mixed_rows: bfloat16 [512, 2048], P(('grp', 'fs'))
- served_gate_before: bfloat16 [2048, 5632], P('grp', 'tp')
- served_up_before: bfloat16 [2048, 5632], P('grp', 'tp')
- served_down_before: bfloat16 [5632, 2048], P(('grp', 'tp'))
- served_gate_after: bfloat16 [2048, 5632], P('grp', 'tp')
- served_up_after: bfloat16 [2048, 5632], P('grp', 'tp')
- served_down_after: bfloat16 [5632, 2048], P(('grp', 'tp'))
All inputs are finite; a program needn't handle non-finite values.
Results may differ from a plain program's by a relative error of at most 0.03.
Values may be sent and summed in bfloat16 or wider, within the bound.
A program may use at most 64 MiB of HBM per device.

v0:
```python
import jax
import jax.numpy as jnp
from jax import lax
from jax.sharding import PartitionSpec as P

EPS = 1e-06


def serve_weights(gain, gate_w, up_w, down_w):
    gate_half = (gain[:, None] * gate_w).astype(jnp.bfloat16)
    up_half = (gain[:, None] * up_w).astype(jnp.bfloat16)
    down_half = down_w.astype(jnp.bfloat16)
    gate_whole, up_whole = (
        lax.all_gather(gate_half, "fs", axis=0, tiled=True),
        lax.all_gather(up_half, "fs", axis=0, tiled=True),
    )
    tall_block = lax.all_gather(down_half, "fs", axis=0, tiled=True)
    down_whole = lax.all_to_all(tall_block, "tp", split_axis=0, concat_axis=1, tiled=True)
    return (gate_whole, up_whole, down_whole)


def half_step(row_block, gate_w, up_w, down_w):
    values = row_block.astype(jnp.float32)
    normed = (values * lax.rsqrt(jnp.mean(values * values, axis=-1, keepdims=True) + EPS)).astype(
        jnp.bfloat16
    )
    gate_pre = jnp.dot(normed, gate_w, preferred_element_type=jnp.float32)
    up_pre = jnp.dot(normed, up_w, preferred_element_type=jnp.float32)
    hidden = (jax.nn.silu(gate_pre) * up_pre).astype(jnp.bfloat16)
    total = lax.psum(
        jnp.dot(hidden, down_w, preferred_element_type=jnp.float32).astype(jnp.bfloat16), "tp"
    ).astype(jnp.float32)
    return (values + 0.5 * total).astype(jnp.bfloat16)


def body(
    prompt_rows,
    gain_before,
    gate_before,
    up_before,
    down_before,
    gain_after,
    gate_after,
    up_after,
    down_after,
):
    gate_one, up_one, down_one = serve_weights(gain_before, gate_before, up_before, down_before)
    gate_two, up_two, down_two = serve_weights(gain_after, gate_after, up_after, down_after)
    middle = half_step(prompt_rows, gate_one, up_one, down_one)
    mixed = half_step(middle, gate_two, up_two, down_two)
    return (mixed, gate_one, up_one, down_one, gate_two, up_two, down_two)


def solution(mesh):
    placed = (
        P(("grp", "fs"), None),
        P("fs"),
        P("fs", "tp"),
        P("fs", "tp"),
        P("fs", "tp"),
        P("fs"),
        P("fs", "tp"),
        P("fs", "tp"),
        P("fs", "tp"),
    )
    return jax.shard_map(
        body,
        mesh=mesh,
        in_specs=placed,
        out_specs=(
            P(("grp", "fs"), None),
            P("grp", "tp"),
            P("grp", "tp"),
            P(("grp", "tp"), None),
            P("grp", "tp"),
            P("grp", "tp"),
            P(("grp", "tp"), None),
        ),
        check_vma=False,
    )
```

profile of v0, /device:TPU:0, one launch (start us, length us, event | category | flops | bytes accessed | tf_op | source)
XLA Modules:
  0.0 390.6 jit_solution(4047119397556258142)
XLA Ops:
  7.2 2.4 convert_element_type.59
  9.8 2.2 multiply_convert_fusion.3
  12.0 26.6 %all-gather.11.cloned.1.call-done = bf16[5632,128]{1,0:T(8,128)(2,1)} async-done(((bf16[2816,128]{1,0:T(8,128)(2,1)}), bf16[5632,128]{1,0:T(8,128)(2,1)}) %all-gather.11.cloned.1.call-update) | async-done | bytes 1441808 | tf_op jit(solution)/shard_map/all_gather | solution.py:17
  38.6 5.6 %all-to-all-start = ((bf16[16,352,128]{2,1,0:T(8,128)(2,1)}), bf16[16,352,128]{2,1,0:T(8,128)(2,1)S(1)}, u32[]{:S(2)}, u32[]{:S(2)}) async-start(bf16[16,352,128]{2,1,0:T(8,128)(2,1)} %bitcast.21), calls=%async_computation | async-start | bytes 2883584 | tf_op jit(solution)/shard_map/all_to_all | solution.py:18
  44.3 2.4 convert_element_type.68
  46.7 0.5 all-gather.9.cloned.1.call-update
  47.2 0.3 fusion
  47.5 18.9 %all-gather.7.cloned.1.call-done = bf16[2048,352]{0,1:T(8,128)(2,1)} async-done(((bf16[1024,352]{0,1:T(8,128)(2,1)}), bf16[2048,352]{0,1:T(8,128)(2,1)}) %all-gather.7.cloned.1.call-update) | async-done | bytes 1441808 | tf_op jit(solution)/shard_map/all_gather | solution.py:14
  66.4 2.0 fusion.14
  68.5 25.8 %all-gather.17.cloned.1.call-done = bf16[5632,128]{1,0:T(8,128)(2,1)} async-done(((bf16[2816,128]{1,0:T(8,128)(2,1)}), bf16[5632,128]{1,0:T(8,128)(2,1)}) %all-gather.17.cloned.1.call-update) | async-done | bytes 1441808 | tf_op jit(solution)/shard_map/all_gather | solution.py:17
  94.3 5.6 %all-to-all-start.1 = ((bf16[16,352,128]{2,1,0:T(8,128)(2,1)}), bf16[16,352,128]{2,1,0:T(8,128)(2,1)S(1)}, u32[]{:S(2)}, u32[]{:S(2)}) async-start(bf16[16,352,128]{2,1,0:T(8,128)(2,1)} %bitcast.20), calls=%async_computation.1 | async-start | bytes 2883584 | tf_op jit(solution)/shard_map/all_to_all | solution.py:18
  100.0 1.3 copy_bitcast_fusion.1
  101.3 20.7 %all-gather.9.cloned.1.call-done = bf16[2048,352]{0,1:T(8,128)(2,1)} async-done(((bf16[1024,352]{0,1:T(8,128)(2,1)}), bf16[2048,352]{0,1:T(8,128)(2,1)}) %all-gather.9.cloned.1.call-update) | async-done | bytes 1441808 | tf_op jit(solution)/shard_map/all_gather | solution.py:15
  122.0 5.3 %convolution_convert_fusion.1 = bf16[256,2048]{1,0:T(8,128)(2,1)} fusion(bf16[352,2048]{1,0:T(8,128)(2,1)} %copy_bitcast_fusion.1, bf16[2048,352]{0,1:T(8,128)(2,1)} %all-gather.9.cloned.1.call-done, bf16[256,2048]{1,0:T(8,128)(2,1)} %param.9, f32[256]{0:T(256)S(1)} %add_rsqrt_fusion.1, f32[256,352]{0,1:T(8,128)S(1)} %fusion.14), kind=kOutput, calls=%fused_computation.7 | convolution fusion | flops 740835328 | bytes 5342208 | tf_op jit(solution)/shard_map/dot_general | solution.py:31
  127.4 2.8 multiply_convert_fusion.1
  130.3 0.7 all-gather.15.cloned.1.call-update
  131.1 1.3 copy_bitcast_fusion
  132.4 89.0 %all-reduce.3.cloned.1.call-done = bf16[256,2048]{1,0:T(8,128)(2,1)} async-done(((bf16[256,2048]{1,0:T(8,128)(2,1)}), bf16[256,2048]{1,0:T(8,128)(2,1)}) %all-reduce.3.cloned.1.call-update) | async-done | bytes 1048592 | tf_op jit(solution)/shard_map/psum | solution.py:30
  221.3 1.8 fusion.3
  223.2 25.0 %all-gather.13.cloned.1.call-done = bf16[2048,352]{0,1:T(8,128)(2,1)} async-done(((bf16[1024,352]{0,1:T(8,128)(2,1)}), bf16[2048,352]{0,1:T(8,128)(2,1)}) %all-gather.13.cloned.1.call-update) | async-done | bytes 1441808 | tf_op jit(solution)/shard_map/all_gather | solution.py:14
  248.1 2.1 fusion.10
  250.3 25.7 %all-gather.15.cloned.1.call-done = bf16[2048,352]{0,1:T(8,128)(2,1)} async-done(((bf16[1024,352]{0,1:T(8,128)(2,1)}), bf16[2048,352]{0,1:T(8,128)(2,1)}) %all-gather.15.cloned.1.call-update) | async-done | bytes 1441808 | tf_op jit(solution)/shard_map/all_gather | solution.py:15
  276.0 4.4 %convolution_convert_fusion = bf16[256,2048]{1,0:T(8,128)(2,1)} fusion(bf16[352,2048]{1,0:T(8,128)(2,1)S(1)} %copy-done.9, bf16[2048,352]{0,1:T(8,128)(2,1)} %all-gather.15.cloned.1.call-done, bf16[256,2048]{1,0:T(8,128)(2,1)S(1)} %get-tuple-element.8, f32[256]{0:T(256)S(1)} %add_rsqrt_fusion, f32[256,352]{0,1:T(8,128)S(1)} %fusion.10), kind=kOutput, calls=%fused_computation.6 | convolution fusion | flops 740835328 | bytes 5342208 | tf_op jit(solution)/shard_map/dot_general | solution.py:31
  280.5 94.0 %all-reduce.5.cloned.1.call-done = bf16[256,2048]{1,0:T(8,128)(2,1)} async-done(((bf16[256,2048]{1,0:T(8,128)(2,1)}), bf16[256,2048]{1,0:T(8,128)(2,1)}) %all-reduce.5.cloned.1.call-update) | async-done | bytes 1048592 | tf_op jit(solution)/shard_map/psum | solution.py:30
  374.4 2.6 fusion.5
  377.0 1.1 copy.30
  378.1 0.8 copy-done.6
  378.9 1.1 copy.31
  380.0 0.8 copy-done.7
  380.8 1.1 copy.32
  381.9 0.8 copy-done.8
  382.7 1.1 copy.33
  (37 shorter events, 0.5 us)
Async XLA Ops:
  7.2 2.6 copy-start.2
  7.2 2.6 copy-start.3
  7.2 31.4 %all-gather.11.cloned.1.call-start = ((), (), s32[]{:S(2)}) async-start(), calls=%async_computation.4 | async-start | bytes 2162688 | tf_op jit(solution)/shard_map/all_gather | solution.py:17
  9.7 56.7 %all-gather.7.cloned.1.call-start = ((), (), s32[]{:S(2)}) async-start(), calls=%async_computation.2 | async-start | bytes 2162688 | tf_op jit(solution)/shard_map/all_gather | solution.py:14
  38.6 55.7 %all-to-all-start = ((bf16[16,352,128]{2,1,0:T(8,128)(2,1)}), bf16[16,352,128]{2,1,0:T(8,128)(2,1)S(1)}, u32[]{:S(2)}, u32[]{:S(2)}) async-start(bf16[16,352,128]{2,1,0:T(8,128)(2,1)} %bitcast.21), calls=%async_computation | async-start | bytes 2883584 | tf_op jit(solution)/shard_map/all_to_all | solution.py:18
  44.2 3.0 copy-start
  44.2 50.1 %all-gather.17.cloned.1.call-start = ((), (), s32[]{:S(2)}) async-start(), calls=%async_computation.8 | async-start | bytes 2162688 | tf_op jit(solution)/shard_map/all_gather | solution.py:17
  46.7 75.4 %all-gather.9.cloned.1.call-start = ((), (), s32[]{:S(2)}) async-start(), calls=%async_computation.3 | async-start | bytes 2162688 | tf_op jit(solution)/shard_map/all_gather | solution.py:15
  94.3 36.8 %all-to-all-start.1 = ((bf16[16,352,128]{2,1,0:T(8,128)(2,1)}), bf16[16,352,128]{2,1,0:T(8,128)(2,1)S(1)}, u32[]{:S(2)}, u32[]{:S(2)}) async-start(bf16[16,352,128]{2,1,0:T(8,128)(2,1)} %bitcast.20), calls=%async_computation.1 | async-start | bytes 2883584 | tf_op jit(solution)/shard_map/all_to_all | solution.py:18
  99.9 121.4 %all-reduce.3.cloned.1.call-start = ((), (), s32[]{:S(2)}) async-start(), calls=%async_computation.5 | async-start | bytes 2097152 | tf_op jit(solution)/shard_map/psum | solution.py:30
  101.3 26.1 %copy-start.10 = (f32[1024]{0:T(1024)S(1)}, f32[1024]{0:T(1024)}, u32[]{:S(2)}) copy-start(f32[1024]{0:T(1024)} %param.14) | copy-start | bytes 12292
  122.0 5.4 %copy-start.4 = (f32[1024,352]{0,1:T(8,128)S(1)}, f32[1024,352]{0,1:T(8,128)}, u32[]{:S(2)}) copy-start(f32[1024,352]{0,1:T(8,128)} %param.15) | copy-start | bytes 4325380
  127.3 120.8 %all-gather.13.cloned.1.call-start = ((), (), s32[]{:S(2)}) async-start(), calls=%async_computation.6 | async-start | bytes 2162688 | tf_op jit(solution)/shard_map/all_gather | solution.py:14
  130.3 145.7 %all-gather.15.cloned.1.call-start = ((), (), s32[]{:S(2)}) async-start(), calls=%async_computation.7 | async-start | bytes 2162688 | tf_op jit(solution)/shard_map/all_gather | solution.py:15
  131.0 90.3 %copy-start.1 = (bf16[256,2048]{1,0:T(8,128)(2,1)S(1)}, bf16[256,2048]{1,0:T(8,128)(2,1)}, u32[]{:S(2)}) copy-start(bf16[256,2048]{1,0:T(8,128)(2,1)} %param.9) | copy-start | bytes 3145732
  131.0 243.4 %all-reduce.5.cloned.1.call-start = ((), (), s32[]{:S(2)}) async-start(), calls=%async_computation.9 | async-start | bytes 2097152 | tf_op jit(solution)/shard_map/psum | solution.py:30
  248.1 27.9 %copy-start.9 = (bf16[352,2048]{1,0:T(8,128)(2,1)S(1)}, bf16[352,2048]{1,0:T(8,128)(2,1)}, u32[]{:S(2)}) copy-start(bf16[352,2048]{1,0:T(8,128)(2,1)} %copy_bitcast_fusion) | copy-start | bytes 4325380
  280.5 96.6 %copy-start.5 = (bf16[2048,352]{0,1:T(8,128)(2,1)S(1)}, bf16[2048,352]{0,1:T(8,128)(2,1)}, u32[]{:S(2)}) copy-start(bf16[2048,352]{0,1:T(8,128)(2,1)} %all-gather.7.cloned.1.call-done) | copy-start | bytes 4325380
  377.0 1.9 copy-start.6
  378.9 1.9 copy-start.7
  380.8 1.9 copy-start.8
Sparse Core Ops, SparseCore 0:
  10.1 28.4 all-gather.10
  40.7 25.6 all-gather.6
  68.6 25.6 all-gather.16
  96.3 25.6 all-gather.8
  127.5 93.8 all-reduce.2
  223.3 24.7 all-gather.12
  250.3 25.6 all-gather.14
  280.6 93.8 all-reduce.4
where the time goes:
time: 391 us
  waiting for transfers between devices  327 us (84%)
  other arithmetic  14.5 us (4%)
  between operations  14.3 us (4%)
  matrix products  13.9 us (4%)
  starting transfers between devices  11.6 us (3%)
  local copies, waits for them, and re-layouts  9.35 us (2%)
    psum x2, waiting for transfers between devices, half_step(): lax.psum(jnp.dot(hidden, down_w, preferred_element_type=jnp.float32).asty...  183 us
    all_gather x2, waiting for transfers between devices, serve_weights(): tall_block = lax.all_gather(down_half, 'fs', axis=0, tiled=True)  52.5 us
    all_gather x2, waiting for transfers between devices, serve_weights(): lax.all_gather(up_half, 'fs', axis=0, tiled=True)  46.5 us
    all_gather x2, waiting for transfers between devices, serve_weights(): lax.all_gather(gate_half, 'fs', axis=0, tiled=True)  43.9 us
    all_to_all x2, starting transfers between devices, serve_weights(): lax.all_to_all(tall_block, 'tp', split_axis=0, concat_axis=1, tiled=True)  11.2 us
    dot_general x2, matrix products, half_step(): jnp.dot(hidden, down_w, preferred_element_type=jnp.float32)  9.75 us
  transfers between devices with their start and end apart: 10, of which 8 were waited for; matrix products, arithmetic and copies ran while one was open for 5% of the time, Pallas kernels for 0%

commit v1 on v0

--- a/solution.py
+++ b/solution.py
@@ -1,7 +1,15 @@
+import functools
+
 import jax
 import jax.numpy as jnp
 from jax import lax
+from jax.experimental import pallas as pl
+from jax.experimental.pallas import tpu as pltpu
 from jax.sharding import PartitionSpec as P
+
+MESH = pl.DeviceIdType.MESH
+BF16 = jnp.bfloat16
+F32 = jnp.float32
 
 EPS = 1e-06
 
@@ -51,6 +59,327 @@
     return (mixed, gate_one, up_one, down_one, gate_two, up_two, down_two)
 
 
+def rows_of(start, size, unit):
+    return pl.ds(pl.multiple_of(start, unit), size)
+
+
+def kernel(
+    n_tp,
+    x_hbm, gain1_hbm, gate1_hbm, up1_hbm, down1_hbm, gain2_hbm, gate2_hbm, up2_hbm, down2_hbm,
+    mixed_hbm, gate1_out, up1_out, down1_out, gate2_out, up2_out, down2_out,
+    x, gain, wide, tall_in, served, tall, down, normed, hidden, part, pair, half, scatter, rows_out,
+    in_sem, out_sem, x_send, x_recv, a_send, a_recv, p_send, p_recv, s_send, s_recv, g_send, g_recv,
+    h_send, h_recv,
+):
+    f = lax.axis_index("fs")
+    t = lax.axis_index("tp")
+    other = 1 - f
+    core = lax.rem(t, 2)
+    chip = t // 2
+    sibling = t + 1 - 2 * core
+    chips = n_tp // 2
+    depth = wide.shape[1]
+    tall_half = tall_in.shape[1]
+    block = down.shape[1]
+    col = tall.shape[2]
+    tokens = x.shape[0]
+    side = tokens // 2
+    piece = side // chips
+    per_half = n_tp // 2
+
+    loads = {}
+    sources = (
+        ("down1", down1_hbm, tall_in.at[0]), ("gain1", gain1_hbm, gain.at[0]),
+        ("gate1", gate1_hbm, wide.at[0]), ("up1", up1_hbm, wide.at[1]),
+        ("down2", down2_hbm, tall_in.at[1]), ("gain2", gain2_hbm, gain.at[1]),
+        ("gate2", gate2_hbm, wide.at[2]), ("up2", up2_hbm, wide.at[3]), ("x", x_hbm, x),
+    )
+    for i, (name, src, dst) in enumerate(sources):
+        loads[name] = pltpu.make_async_copy(src, dst, in_sem.at[i])
+        loads[name].start()
+
+    barrier = pltpu.get_barrier_semaphore()
+    for k in range(1, n_tp):
+        pl.semaphore_signal(
+            barrier, inc=1, device_id={"fs": f, "tp": lax.rem(t + k, n_tp)}, device_id_type=MESH
+        )
+    pl.semaphore_signal(barrier, inc=1, device_id={"fs": other, "tp": t}, device_id_type=MESH)
+    pl.semaphore_wait(barrier, n_tp)
+
+    def across(ref, slot):
+        return pltpu.make_async_remote_copy(
+            src_ref=ref, dst_ref=ref, send_sem=x_send.at[slot], recv_sem=x_recv.at[slot],
+            device_id={"fs": other, "tp": t}, device_id_type=MESH,
+        )
+
+    def fold_wide(i, gain_slot):
+        step = depth // 8
+
+        def one(k, _):
+            rows = rows_of(k * step, step, step)
+            value = gain[gain_slot, rows, :] * wide[i, rows, :]
+            served[i, rows_of(f * depth + k * step, step, step), :] = value.astype(BF16)
+            return 0
+
+        lax.fori_loop(0, 8, one, 0)
+        sent = across(served.at[i, rows_of(f * depth, depth, depth)], i)
+        sent.start()
+        return sent
+
+    def fold_tall(layer):
+        step = tall_half // 8
+
+        def one(k, _):
+            tall[layer, rows_of(f * tall_half + k * step, step, 16), :] = tall_in[
+                layer, rows_of(k * step, step, 16), :
+            ].astype(BF16)
+            return 0
+
+        lax.fori_loop(0, 8, one, 0)
+        sent = across(tall.at[layer, rows_of(f * tall_half, tall_half, 16)], 4 + layer)
+        sent.start()
+        return sent
+
+    my_cols = pl.ds(pl.multiple_of(t * col, col), col)
+
+    def block_copy(layer, b, sender):
+        return pltpu.make_async_remote_copy(
+            src_ref=tall.at[layer, rows_of(b * block, block, 16)],
+            dst_ref=down.at[layer, :, my_cols],
+            send_sem=a_send.at[layer, b], recv_sem=a_recv.at[layer, sender],
+            device_id={"fs": f, "tp": b}, device_id_type=MESH,
+        )
+
+    def hand_out(layer, which):
+        def one(k, _):
+            b = which * per_half + lax.rem(t + k, per_half)
+
+            @pl.when(b != t)
+            def _():
+                block_copy(layer, b, t).start()
+
+            return 0
+
+        lax.fori_loop(0, per_half, one, 0)
+
+    def collect(layer):
+        def one(k, _):
+            block_copy(layer, t, lax.rem(t + k, n_tp)).wait_recv()
+            return 0
+
+        lax.fori_loop(1, n_tp, one, 0)
+        down[layer, :, my_cols] = tall[layer, rows_of(t * block, block, 16), :]
+
+    outs = []
+
+    def put(src, dst):
+        copy = pltpu.make_async_copy(src, dst, out_sem.at[len(outs)])
+        copy.start()
+        outs.append(copy)
+
+    sends = []
+    loads["down1"].wait()
+    tall_one = fold_tall(0)
+    hand_out(0, f)
+    loads["gain1"].wait()
+    loads["gate1"].wait()
+    gate_one = fold_wide(0, 0)
+    loads["up1"].wait()
+    up_one = fold_wide(1, 0)
+    loads["down2"].wait()
+    tall_two = fold_tall(1)
+    loads["gain2"].wait()
+    loads["gate2"].wait()
+    gate_two = fold_wide(2, 1)
+    loads["up2"].wait()
+    up_two = fold_wide(3, 1)
+    loads["x"].wait()
+
+    def norm(src):
+        def one(k, _):
+            rows = rows_of(k * 32, 32, 32)
+            v = src[rows, :].astype(F32)
+            scale = lax.rsqrt(jnp.mean(v * v, axis=-1, keepdims=True) + EPS)
+            normed[rows, :] = (v * scale).astype(BF16)
+            return 0
+
+        lax.fori_loop(0, tokens // 32, one, 0)
+
+    norm(x)
+    tall_one.wait_recv()
+    hand_out(0, other)
+    hand_out(1, f)
+
+    def hide(layer):
+        gate, up = served.at[2 * layer], served.at[2 * layer + 1]
+        step = tokens // 2
+
+        def one(k, _):
+            rows = rows_of(k * step, step, step)
+            v = normed[rows, :]
+            g = jnp.dot(v, gate[...], preferred_element_type=F32)
+            u = jnp.dot(v, up[...], preferred_element_type=F32)
+            hidden[rows, :] = (g / (1.0 + jnp.exp(-g)) * u).astype(BF16)
+            return 0
+
+        lax.fori_loop(0, 2, one, 0)
+
+    def project(layer):
+        step = tokens // 2
+
+        def one(k, _):
+            rows = rows_of(k * step, step, step)
+            p = jnp.dot(hidden[rows, :], down[layer], preferred_element_type=F32)
+            part[layer, rows, :] = p.astype(BF16)
+            return 0
+
+        lax.fori_loop(0, 2, one, 0)
+
+    def chip_copy(src, dst, send, recv, q, sem_at, layer):
+        return pltpu.make_async_remote_copy(
+            src_ref=src, dst_ref=dst, send_sem=send.at[layer, q], recv_sem=recv.at[layer, sem_at],
+            device_id={"fs": f, "tp": 2 * q + core}, device_id_type=MESH,
+        )
+
+    def to_sibling(src, dst, send, recv, layer):
+        return pltpu.make_async_remote_copy(
+            src_ref=src, dst_ref=dst, send_sem=send.at[layer], recv_sem=recv.at[layer],
+            device_id={"fs": f, "tp": sibling}, device_id_type=MESH,
+        )
+
+    def scatter_copy(layer, q, sender):
+        return chip_copy(
+            half.at[layer, rows_of(q * piece, piece, piece)], scatter.at[layer, sender],
+            s_send, s_recv, q, sender, layer,
+        )
+
+    mine = rows_of(core * side + chip * piece, piece, piece)
+
+    def gather_copy(layer, q, sender):
+        ref = rows_out.at[layer, mine]
+        return chip_copy(ref, ref, g_send, g_recv, q, sender, layer)
+
+    def for_chips(act):
+        def one(k, _):
+            act(lax.rem(chip + k, chips))
+            return 0
+
+        lax.fori_loop(1, chips, one, 0)
+
+    def add_up(layer, base, between):
+        swap = to_sibling(
+            part.at[layer, rows_of((1 - core) * side, side, side)], pair.at[layer], p_send, p_recv, layer
+        )
+        swap.start()
+        swap.wait_recv()
+
+        def add(k, _):
+            rows = rows_of(k * piece, piece, piece)
+            own = part[layer, rows_of(core * side + k * piece, piece, piece), :].astype(F32)
+            half[layer, rows, :] = (own + pair[layer, rows, :].astype(F32)).astype(BF16)
+            return 0
+
+        lax.fori_loop(0, chips, add, 0)
+        for_chips(lambda q: scatter_copy(layer, q, chip).start())
+        for_chips(lambda q: scatter_copy(layer, chip, q).wait_recv())
+        scatter[layer, chip] = half[layer, rows_of(chip * piece, piece, piece), :]
+        total = scatter[layer, 0].astype(F32)
+        for q in range(1, chips):
+            total = total + scatter[layer, q].astype(F32)
+        rows_out[layer, mine, :] = (base[mine, :].astype(F32) + 0.5 * total).astype(BF16)
+        for_chips(lambda q: gather_copy(layer, q, chip).start())
+        between()
+        for_chips(lambda q: gather_copy(layer, chip, q).wait_recv())
+        ref = rows_out.at[layer, rows_of(core * side, side, side)]
+        fill = to_sibling(ref, ref, h_send, h_recv, layer)
+        fill.start()
+        fill.wait_recv()
+        sends.extend((swap, fill))
+
+    gate_one.wait_recv()
+    up_one.wait_recv()
+    put(served.at[0], gate1_out)
+    put(served.at[1], up1_out)
+    hide(0)
+    collect(0)
+    put(down.at[0], down1_out)
+    project(0)
+
+    def relay():
+        tall_two.wait_recv()
+        hand_out(1, other)
+
+    add_up(0, x, relay)
+    norm(rows_out.at[0])
+    gate_two.wait_recv()
+    up_two.wait_recv()
+    put(served.at[2], gate2_out)
+    put(served.at[3], up2_out)
+    hide(1)
+    collect(1)
+    put(down.at[1], down2_out)
+    project(1)
+    add_up(1, rows_out.at[0], lambda: None)
+    put(rows_out.at[1], mixed_hbm)
+
+    for sent in (tall_one, gate_one, up_one, tall_two, gate_two, up_two, *sends):
+        sent.wait_send()
+    for layer in range(2):
+
+        def drain(k, _):
+            block_copy(layer, lax.rem(t + k, n_tp), t).wait_send()
+            return 0
+
+        lax.fori_loop(1, n_tp, drain, 0)
+        for_chips(lambda q: scatter_copy(layer, q, chip).wait_send())
+        for_chips(lambda q: gather_copy(layer, q, chip).wait_send())
+    for copy in outs:
+        copy.wait()
+
+
+def fused(n_tp, x, gain1, gate1, up1, down1, gain2, gate2, up2, down2):
+    depth, width = gate1.shape
+    tall_half, col = down1.shape
+    tokens, model = x.shape
+    block = 2 * tall_half // n_tp
+    chips = n_tp // 2
+    side = tokens // 2
+    dma = pltpu.SemaphoreType.DMA
+    shape = jax.ShapeDtypeStruct
+    anywhere = pl.BlockSpec(memory_space=pl.ANY)
+    wide_out = shape((2 * depth, width), BF16)
+    down_out = shape((block, model), BF16)
+    return pl.pallas_call(
+        functools.partial(kernel, n_tp),
+        out_shape=(shape(x.shape, BF16), wide_out, wide_out, down_out, wide_out, wide_out, down_out),
+        in_specs=[anywhere] * 9,
+        out_specs=[anywhere] * 7,
+        scratch_shapes=[
+            pltpu.VMEM((tokens, model), BF16),
+            pltpu.VMEM((2, depth, 1), F32),
+            pltpu.VMEM((4, depth, width), F32),
+            pltpu.VMEM((2, tall_half, col), F32),
+            pltpu.VMEM((4, 2 * depth, width), BF16),
+            pltpu.VMEM((2, 2 * tall_half, col), BF16),
+            pltpu.VMEM((2, block, model), BF16),
+            pltpu.VMEM((tokens, model), BF16),
+            pltpu.VMEM((tokens, width), BF16),
+            pltpu.VMEM((2, tokens, model), BF16),
+            pltpu.VMEM((2, side, model), BF16),
+            pltpu.VMEM((2, side, model), BF16),
+            pltpu.VMEM((2, chips, side // chips, model), BF16),
+            pltpu.VMEM((2, tokens, model), BF16),
+            dma((9,)), dma((7,)), dma((6,)), dma((6,)), dma((2, n_tp)), dma((2, n_tp)),
+            dma((2,)), dma((2,)), dma((2, chips)), dma((2, chips)), dma((2, chips)), dma((2, chips)),
+            dma((2,)), dma((2,)),
+        ],
+        compiler_params=pltpu.CompilerParams(
+            collective_id=0, has_side_effects=True, vmem_limit_bytes=56 * 1024 * 1024
+        ),
+        name="hand_over",
+    )(x, gain1[:, None], gate1, up1, down1, gain2[:, None], gate2, up2, down2)
+
+
 def solution(mesh):
     placed = (
         P(("grp", "fs"), None),
@@ -63,8 +392,9 @@
         P("fs", "tp"),
         P("fs", "tp"),
     )
+    paired = mesh.shape["fs"] == 2 and mesh.shape["tp"] % 4 == 0
     return jax.shard_map(
-        body,
+        functools.partial(fused, mesh.shape["tp"]) if paired else body,
         mesh=mesh,
         in_specs=placed,
         out_specs=(

time: 391 us -> 189 us (0.48)
  waiting for transfers between devices: 327 us -> 0 us
  Pallas kernels: 0 us -> 161 us
  other arithmetic: 14.5 us -> 0 us
  local copies, waits for them, and re-layouts: 9.35 us -> 23.5 us
  matrix products: 13.9 us -> 0 us
  between operations: 14.3 us -> 0.66 us
  starting transfers between devices: 11.6 us -> 0 us
    psum x2 -> x0, waiting for transfers between devices: 183 us -> none  [half_step(): lax.psum(jnp.dot(hidden, down_w, preferred_element_type=jnp.float32).asty...]
    pallas_call x0 -> x1, Pallas kernels: none -> 161 us  [fused(): pl.pallas_call(functools.partial(kernel, n_tp), out_shape=(shape(x.shape,...]
    all_gather x6 -> x0, waiting for transfers between devices: 143 us -> none  [the longest x2 52.5 us: serve_weights(): tall_block = lax.all_gather(down_half, 'fs', axis=0, tiled=True)]
    dot_general x4 -> x0, matrix products: 13.9 us -> none  [the longest x2 9.75 us: half_step(): jnp.dot(hidden, down_w, preferred_element_type=jnp.float32)]
    convert_element_type x5 -> x0, other arithmetic: 12.4 us -> none  [the longest x2 4.98 us: serve_weights(): gate_half = (gain[:, None] * gate_w).astype(jnp.bfloat16)]
    all_to_all x2 -> x0, starting transfers between devices: 11.2 us -> none  [serve_weights(): lax.all_to_all(tall_block, 'tp', split_axis=0, concat_axis=1, tiled=True)]
    pallas_call x0 -> x4, local copies, waits for them, and re-layouts: none -> 7.39 us  [fused(): pl.pallas_call(functools.partial(kernel, n_tp), out_shape=(shape(x.shape,...]
    unnamed x26 -> x25, local copies, waits for them, and re-layouts: 6.78 us -> 12.7 us
  transfers between devices with their start and end apart: 10 -> 0, of which waited for: 8 -> 0; matrix products, arithmetic and copies ran while one was open for 5% -> 0% of each run, Pallas kernels for 0% -> 0%
where the time goes in v1:
time: 189 us; the launch traced here: 185 us
  Pallas kernels  161 us (85%)
  local copies, waits for them, and re-layouts  23.5 us (12%)
    pallas_call x1, Pallas kernels, fused(): pl.pallas_call(functools.partial(kernel, n_tp), out_shape=(shape(x.shape,...  161 us
    unnamed x25, local copies, waits for them, and re-layouts  12.7 us
    pallas_call x4, local copies, waits for them, and re-layouts, fused(): pl.pallas_call(functools.partial(kernel, n_tp), out_shape=(shape(x.shape,...  7.39 us

profile of v1, /device:TPU:0, one launch (start us, length us, event | category | flops | bytes accessed | tf_op | source)
XLA Modules:
  0.0 185.1 jit_solution(16931702370487043232)
XLA Ops:
  0.6 1.7 copy.24.gain1_hbm
  2.3 1.7 copy.27.gain2_hbm
  4.0 0.0 copy-start.3
  4.0 3.1 %copy.25.gate1_hbm = f32[1024,352]{1,0:T(8,128)} copy(f32[1024,352]{0,1:T(8,128)} %param.11) | data formatting | bytes 2883584 | tf_op args[2]
  7.1 0.0 copy-done.3
  7.1 0.0 copy-start.4
  7.1 1.6 copy.26.up1_hbm
  8.8 0.0 copy-done.4
  8.8 0.0 copy-start.5
  8.8 1.6 copy.28.gate2_hbm
  10.4 0.0 copy-done.5
  10.4 1.6 copy.29.up2_hbm
  12.0 160.9 %hand_over.1 = (bf16[256,2048]{1,0:T(8,128)(2,1)}, bf16[2048,352]{1,0:T(8,128)(2,1)}, bf16[2048,352]{1,0:T(8,128)(2,1)}, bf16[352,2048]{1,0:T(8,128)(2,1)}, bf16...) custom-call(bf16[256,2048]{1,0:T(8,128)(2,1)} %x_hbm.1, f32[1024,1]{1,0:T(8,128)} %copy.24.gain1_hbm, ...), custom_call_target="tpu_custom_call" | custom-call | tf_op jit(solution)/shard_map/hand_over/pallas_call | solution.py:352
  172.9 0.0 copy-start.2
  172.9 2.7 %copy.30 = bf16[2048,352]{0,1:T(8,128)(2,1)} copy(bf16[2048,352]{1,0:T(8,128)(2,1)} %get-tuple-element.15) | data formatting | bytes 2883584 | tf_op jit(solution)/shard_map/hand_over/pallas_call | solution.py:352
  175.6 0.0 copy-done.2
  175.6 0.0 copy-start.1
  175.6 1.6 copy.31
  177.2 0.0 copy-done.1
  177.2 0.0 copy-start
  177.2 1.6 copy.32
  178.7 0.0 copy-done
  178.8 0.0 copy-start.8
  178.8 1.6 copy.33
  180.3 0.0 copy-done.8
  180.3 0.0 copy-start.7
  180.3 1.0 copy.37
  181.3 0.8 copy-done.7
  182.1 0.0 copy-start.6
  182.1 1.1 copy.38
  183.2 0.8 copy-done.6
  184.0 1.1 copy.39
Async XLA Ops:
  4.0 3.1 %copy-start.3 = (f32[1024,352]{0,1:T(8,128)S(1)}, f32[1024,352]{0,1:T(8,128)}, u32[]{:S(2)}) copy-start(f32[1024,352]{0,1:T(8,128)} %param.12) | copy-start | bytes 4325380
  7.1 1.6 copy-start.4
  8.8 1.6 copy-start.5
  172.9 2.7 %copy-start.2 = (bf16[2048,352]{1,0:T(8,128)(2,1)S(1)}, bf16[2048,352]{1,0:T(8,128)(2,1)}, u32[]{:S(2)}) copy-start(bf16[2048,352]{1,0:T(8,128)(2,1)} %get-tuple-element.16) | copy-start | bytes 4325380
  175.6 1.6 copy-start.1
  177.2 1.6 copy-start
  178.8 1.6 copy-start.8
  180.3 1.7 copy-start.7
  182.1 1.9 %copy-start.6 = (bf16[352,2048]{1,0:T(8,128)(2,1)S(1)}, bf16[352,2048]{1,0:T(8,128)(2,1)}, u32[]{:S(2)}) copy-start(bf16[352,2048]{1,0:T(8,128)(2,1)} %get-tuple-element.34) | copy-start | bytes 4325380

commit v2 on v1

--- a/solution.py
+++ b/solution.py
@@ -78,7 +78,7 @@
     chip = t // 2
     sibling = t + 1 - 2 * core
     chips = n_tp // 2
-    depth = wide.shape[1]
+    width, depth = wide.shape[1:]
     tall_half = tall_in.shape[1]
     block = down.shape[1]
     col = tall.shape[2]
@@ -112,19 +112,16 @@
             device_id={"fs": other, "tp": t}, device_id_type=MESH,
         )
 
+    near = rows_of(f * depth, depth, depth)
+
     def fold_wide(i, gain_slot):
-        step = depth // 8
-
-        def one(k, _):
-            rows = rows_of(k * step, step, step)
-            value = gain[gain_slot, rows, :] * wide[i, rows, :]
-            served[i, rows_of(f * depth + k * step, step, step), :] = value.astype(BF16)
-            return 0
-
-        lax.fori_loop(0, 8, one, 0)
-        sent = across(served.at[i, rows_of(f * depth, depth, depth)], i)
-        sent.start()
-        return sent
+        def one(k, _):
+            rows = rows_of(k * 32, 32, 32)
+            served[i, rows, near] = (gain[gain_slot] * wide[i, rows, :]).astype(BF16)
+            return 0
+
+        lax.fori_loop(0, width // 32, one, 0)
+        return across(served.at[i, :, near], i)
 
     def fold_tall(layer):
         step = tall_half // 8
@@ -136,9 +133,7 @@
             return 0
 
         lax.fori_loop(0, 8, one, 0)
-        sent = across(tall.at[layer, rows_of(f * tall_half, tall_half, 16)], 4 + layer)
-        sent.start()
-        return sent
+        return across(tall.at[layer, rows_of(f * tall_half, tall_half, 16)], 4 + layer)
 
     my_cols = pl.ds(pl.multiple_of(t * col, col), col)
 
@@ -180,14 +175,17 @@
     sends = []
     loads["down1"].wait()
     tall_one = fold_tall(0)
+    tall_one.start()
     hand_out(0, f)
+    loads["down2"].wait()
+    tall_two = fold_tall(1)
+    tall_two.start()
+    hand_out(1, f)
     loads["gain1"].wait()
     loads["gate1"].wait()
     gate_one = fold_wide(0, 0)
     loads["up1"].wait()
     up_one = fold_wide(1, 0)
-    loads["down2"].wait()
-    tall_two = fold_tall(1)
     loads["gain2"].wait()
     loads["gate2"].wait()
     gate_two = fold_wide(2, 1)
@@ -207,8 +205,13 @@
 
     norm(x)
     tall_one.wait_recv()
+    gate_one.start()
     hand_out(0, other)
-    hand_out(1, f)
+    tall_two.wait_recv()
+    up_one.start()
+    hand_out(1, other)
+
+    turned = (((1,), (1,)), ((), ()))
 
     def hide(layer):
         gate, up = served.at[2 * layer], served.at[2 * layer + 1]
@@ -217,8 +220,8 @@
         def one(k, _):
             rows = rows_of(k * step, step, step)
             v = normed[rows, :]
-            g = jnp.dot(v, gate[...], preferred_element_type=F32)
-            u = jnp.dot(v, up[...], preferred_element_type=F32)
+            g = lax.dot_general(v, gate[...], turned, preferred_element_type=F32)
+            u = lax.dot_general(v, up[...], turned, preferred_element_type=F32)
             hidden[rows, :] = (g / (1.0 + jnp.exp(-g)) * u).astype(BF16)
             return 0
 
@@ -266,7 +269,7 @@
 
         lax.fori_loop(1, chips, one, 0)
 
-    def add_up(layer, base, between):
+    def add_up(layer, base):
         swap = to_sibling(
             part.at[layer, rows_of((1 - core) * side, side, side)], pair.at[layer], p_send, p_recv, layer
         )
@@ -288,7 +291,6 @@
             total = total + scatter[layer, q].astype(F32)
         rows_out[layer, mine, :] = (base[mine, :].astype(F32) + 0.5 * total).astype(BF16)
         for_chips(lambda q: gather_copy(layer, q, chip).start())
-        between()
         for_chips(lambda q: gather_copy(layer, chip, q).wait_recv())
         ref = rows_out.at[layer, rows_of(core * side, side, side)]
         fill = to_sibling(ref, ref, h_send, h_recv, layer)
@@ -297,19 +299,16 @@
         sends.extend((swap, fill))
 
     gate_one.wait_recv()
+    gate_two.start()
+    put(served.at[0], gate1_out)
     up_one.wait_recv()
-    put(served.at[0], gate1_out)
+    up_two.start()
     put(served.at[1], up1_out)
     hide(0)
     collect(0)
     put(down.at[0], down1_out)
     project(0)
-
-    def relay():
-        tall_two.wait_recv()
-        hand_out(1, other)
-
-    add_up(0, x, relay)
+    add_up(0, x)
     norm(rows_out.at[0])
     gate_two.wait_recv()
     up_two.wait_recv()
@@ -319,7 +318,7 @@
     collect(1)
     put(down.at[1], down2_out)
     project(1)
-    add_up(1, rows_out.at[0], lambda: None)
+    add_up(1, rows_out.at[0])
     put(rows_out.at[1], mixed_hbm)
 
     for sent in (tall_one, gate_one, up_one, tall_two, gate_two, up_two, *sends):
@@ -347,19 +346,19 @@
     dma = pltpu.SemaphoreType.DMA
     shape = jax.ShapeDtypeStruct
     anywhere = pl.BlockSpec(memory_space=pl.ANY)
-    wide_out = shape((2 * depth, width), BF16)
+    wide_out = shape((width, 2 * depth), BF16)
     down_out = shape((block, model), BF16)
-    return pl.pallas_call(
+    mixed, gate_one, up_one, down_one, gate_two, up_two, down_two = pl.pallas_call(
         functools.partial(kernel, n_tp),
         out_shape=(shape(x.shape, BF16), wide_out, wide_out, down_out, wide_out, wide_out, down_out),
         in_specs=[anywhere] * 9,
         out_specs=[anywhere] * 7,
         scratch_shapes=[
             pltpu.VMEM((tokens, model), BF16),
-            pltpu.VMEM((2, depth, 1), F32),
-            pltpu.VMEM((4, depth, width), F32),
+            pltpu.VMEM((2, 1, depth), F32),
+            pltpu.VMEM((4, width, depth), F32),
             pltpu.VMEM((2, tall_half, col), F32),
-            pltpu.VMEM((4, 2 * depth, width), BF16),
+            pltpu.VMEM((4, width, 2 * depth), BF16),
             pltpu.VMEM((2, 2 * tall_half, col), BF16),
             pltpu.VMEM((2, block, model), BF16),
             pltpu.VMEM((tokens, model), BF16),
@@ -377,7 +376,8 @@
             collective_id=0, has_side_effects=True, vmem_limit_bytes=56 * 1024 * 1024
         ),
         name="hand_over",
-    )(x, gain1[:, None], gate1, up1, down1, gain2[:, None], gate2, up2, down2)
+    )(x, gain1[None, :], gate1.T, up1.T, down1, gain2[None, :], gate2.T, up2.T, down2)
+    return (mixed, gate_one.T, up_one.T, down_one, gate_two.T, up_two.T, down_two)
 
 
 def solution(mesh):

time: 189 us -> 164 us (0.87); the launches traced: 185 us -> 163 us
  Pallas kernels: 161 us -> 149 us
  local copies, waits for them, and re-layouts: 23.5 us -> 12.9 us
    pallas_call x1, Pallas kernels: 161 us -> 149 us  [fused(): pl.pallas_call(functools.partial(kernel, n_tp), out_shape=(shape(x.shape,...]
    pallas_call x4 -> x0, local copies, waits for them, and re-layouts: 7.39 us -> none  [fused(): pl.pallas_call(functools.partial(kernel, n_tp), out_shape=(shape(x.shape,...]
    broadcast_in_dim x2 -> x0, local copies, waits for them, and re-layouts: 3.41 us -> none  [the longest x1 1.71 us: fused(): gain1[:, None]]
    unnamed x25 -> x19, local copies, waits for them, and re-layouts: 12.7 us -> 12.9 us
where the time goes in v2:
time: 164 us; the launch traced here: 163 us
  Pallas kernels  149 us (91%)
  local copies, waits for them, and re-layouts  12.9 us (8%)
    pallas_call x1, Pallas kernels, fused(): pl.pallas_call(functools.partial(kernel, n_tp), out_shape=(shape(x.shape,...  149 us
    unnamed x19, local copies, waits for them, and re-layouts  12.9 us

profile of v2, /device:TPU:0, one launch (start us, length us, event | category | flops | bytes accessed | tf_op | source)
XLA Modules:
  0.0 162.6 jit_solution(15162208719047256848)
XLA Ops:
  0.6 149.0 %hand_over.1 = (bf16[256,2048]{1,0:T(8,128)(2,1)}, bf16[352,2048]{1,0:T(8,128)(2,1)}, bf16[352,2048]{1,0:T(8,128)(2,1)}, bf16[352,2048]{1,0:T(8,128)(2,1)}, bf16...) custom-call(bf16[256,2048]{1,0:T(8,128)(2,1)} %x_hbm.1, f32[1,1024]{1,0:T(1,128)} %bitcast.18, ...), custom_call_target="tpu_custom_call" | custom-call | tf_op jit(solution)/shard_map/hand_over/pallas_call | solution.py:351
  149.6 0.0 copy-start.5
  149.6 2.4 %copy.23 = bf16[256,2048]{1,0:T(8,128)(2,1)} copy(bf16[256,2048]{1,0:T(8,128)(2,1)} %get-tuple-element.28) | data formatting | bytes 2097152
  152.0 0.0 copy-done.5
  152.0 0.0 copy-start.4
  152.0 1.1 copy.24
  153.1 0.8 copy-done.4
  153.9 0.0 copy-start.3
  153.9 1.1 copy.25
  155.0 0.8 copy-done.3
  155.8 0.0 copy-start.2
  155.8 1.1 copy.26
  156.9 0.8 copy-done.2
  157.7 0.0 copy-start.1
  157.7 1.1 copy.27
  158.8 0.8 copy-done.1
  159.6 0.0 copy-start
  159.6 1.1 copy.28
  160.7 0.8 copy-done
  161.5 1.1 copy.29
Async XLA Ops:
  149.6 2.4 %copy-start.5 = (bf16[352,2048]{1,0:T(8,128)(2,1)S(1)}, bf16[352,2048]{1,0:T(8,128)(2,1)}, u32[]{:S(2)}) copy-start(bf16[352,2048]{1,0:T(8,128)(2,1)} %get-tuple-element.15) | copy-start | bytes 4325380
  152.0 1.9 %copy-start.4 = (bf16[352,2048]{1,0:T(8,128)(2,1)S(1)}, bf16[352,2048]{1,0:T(8,128)(2,1)}, u32[]{:S(2)}) copy-start(bf16[352,2048]{1,0:T(8,128)(2,1)} %get-tuple-element.16) | copy-start | bytes 4325380
  153.9 1.9 %copy-start.3 = (bf16[352,2048]{1,0:T(8,128)(2,1)S(1)}, bf16[352,2048]{1,0:T(8,128)(2,1)}, u32[]{:S(2)}) copy-start(bf16[352,2048]{1,0:T(8,128)(2,1)} %get-tuple-element.31) | copy-start | bytes 4325380
  155.8 1.9 %copy-start.2 = (bf16[352,2048]{1,0:T(8,128)(2,1)S(1)}, bf16[352,2048]{1,0:T(8,128)(2,1)}, u32[]{:S(2)}) copy-start(bf16[352,2048]{1,0:T(8,128)(2,1)} %get-tuple-element.18) | copy-start | bytes 4325380
  157.7 1.9 %copy-start.1 = (bf16[352,2048]{1,0:T(8,128)(2,1)S(1)}, bf16[352,2048]{1,0:T(8,128)(2,1)}, u32[]{:S(2)}) copy-start(bf16[352,2048]{1,0:T(8,128)(2,1)} %get-tuple-element.19) | copy-start | bytes 4325380
  159.6 1.9 %copy-start = (bf16[352,2048]{1,0:T(8,128)(2,1)S(1)}, bf16[352,2048]{1,0:T(8,128)(2,1)}, u32[]{:S(2)}) copy-start(bf16[352,2048]{1,0:T(8,128)(2,1)} %get-tuple-element.34) | copy-start | bytes 4325380

commit v3 on v2

--- a/solution.py
+++ b/solution.py
@@ -250,13 +250,20 @@
             device_id={"fs": f, "tp": sibling}, device_id_type=MESH,
         )
 
+    lanes = chips // 2
+    lane = lax.rem(chip, 2)
+    beside = chip + 1 - 2 * lane
+
+    def place(q):
+        return lax.rem(q, 2) * lanes + q // 2
+
     def scatter_copy(layer, q, sender):
         return chip_copy(
-            half.at[layer, rows_of(q * piece, piece, piece)], scatter.at[layer, sender],
+            half.at[layer, rows_of(place(q) * piece, piece, piece)], scatter.at[layer, sender],
             s_send, s_recv, q, sender, layer,
         )
 
-    mine = rows_of(core * side + chip * piece, piece, piece)
+    mine = rows_of(core * side + place(chip) * piece, piece, piece)
 
     def gather_copy(layer, q, sender):
         ref = rows_out.at[layer, mine]
@@ -268,6 +275,17 @@
             return 0
 
         lax.fori_loop(1, chips, one, 0)
+
+    def for_lane(act):
+        def one(k, _):
+            act(2 * lax.rem(chip // 2 + k, lanes) + lane)
+            return 0
+
+        lax.fori_loop(1, lanes, one, 0)
+
+    def beside_copy(layer, sender):
+        ref = rows_out.at[layer, rows_of(core * side + lane * (side // 2), side // 2, side // 2)]
+        return chip_copy(ref, ref, g_send, g_recv, beside, sender, layer)
 
     def add_up(layer, base):
         swap = to_sibling(
@@ -285,13 +303,17 @@
         lax.fori_loop(0, chips, add, 0)
         for_chips(lambda q: scatter_copy(layer, q, chip).start())
         for_chips(lambda q: scatter_copy(layer, chip, q).wait_recv())
-        scatter[layer, chip] = half[layer, rows_of(chip * piece, piece, piece), :]
+        scatter[layer, chip] = half[layer, rows_of(place(chip) * piece, piece, piece), :]
         total = scatter[layer, 0].astype(F32)
         for q in range(1, chips):
             total = total + scatter[layer, q].astype(F32)
         rows_out[layer, mine, :] = (base[mine, :].astype(F32) + 0.5 * total).astype(BF16)
-        for_chips(lambda q: gather_copy(layer, q, chip).start())
-        for_chips(lambda q: gather_copy(layer, chip, q).wait_recv())
+        spread = for_chips if layer else for_lane
+        spread(lambda q: gather_copy(layer, q, chip).start())
+        spread(lambda q: gather_copy(layer, chip, q).wait_recv())
+        if layer == 0:
+            beside_copy(layer, chip).start()
+            beside_copy(layer, beside).wait_recv()
         ref = rows_out.at[layer, rows_of(core * side, side, side)]
         fill = to_sibling(ref, ref, h_send, h_recv, layer)
         fill.start()
@@ -331,7 +353,11 @@
 
         lax.fori_loop(1, n_tp, drain, 0)
         for_chips(lambda q: scatter_copy(layer, q, chip).wait_send())
-        for_chips(lambda q: gather_copy(layer, q, chip).wait_send())
+        if layer == 0:
+            for_lane(lambda q: gather_copy(layer, q, chip).wait_send())
+            beside_copy(layer, chip).wait_send()
+        else:
+            for_chips(lambda q: gather_copy(layer, q, chip).wait_send())
     for copy in outs:
         copy.wait()
 

time: 164 us -> 161 us (0.982)
  Pallas kernels: 149 us -> 145 us
    pallas_call x1, Pallas kernels: 149 us -> 145 us  [fused(): pl.pallas_call(functools.partial(kernel, n_tp), out_shape=(shape(x.shape,...]
where the time goes in v3:
time: 161 us; the launch traced here: 159 us
  Pallas kernels  145 us (90%)
  local copies, waits for them, and re-layouts  12.9 us (8%)
    pallas_call x1, Pallas kernels, fused(): pl.pallas_call(functools.partial(kernel, n_tp), out_shape=(shape(x.shape,...  145 us
    unnamed x19, local copies, waits for them, and re-layouts  12.9 us

profile of v3, /device:TPU:0, one launch (start us, length us, event | category | flops | bytes accessed | tf_op | source)
XLA Modules:
  0.0 158.6 jit_solution(91462399750558834)
XLA Ops:
  0.6 145.0 %hand_over.1 = (bf16[256,2048]{1,0:T(8,128)(2,1)}, bf16[352,2048]{1,0:T(8,128)(2,1)}, bf16[352,2048]{1,0:T(8,128)(2,1)}, bf16[352,2048]{1,0:T(8,128)(2,1)}, bf16...) custom-call(bf16[256,2048]{1,0:T(8,128)(2,1)} %x_hbm.1, f32[1,1024]{1,0:T(1,128)} %bitcast.18, ...), custom_call_target="tpu_custom_call" | custom-call | tf_op jit(solution)/shard_map/hand_over/pallas_call | solution.py:377
  145.6 0.0 copy-start.5
  145.6 2.4 %copy.23 = bf16[256,2048]{1,0:T(8,128)(2,1)} copy(bf16[256,2048]{1,0:T(8,128)(2,1)} %get-tuple-element.28) | data formatting | bytes 2097152
  148.1 0.0 copy-done.5
  148.1 0.0 copy-start.4
  148.1 1.1 copy.24
  149.2 0.8 copy-done.4
  149.9 0.0 copy-start.3
  149.9 1.1 copy.25
  151.0 0.8 copy-done.3
  151.8 0.0 copy-start.2
  151.8 1.1 copy.26
  152.9 0.8 copy-done.2
  153.7 0.0 copy-start.1
  153.7 1.1 copy.27
  154.8 0.8 copy-done.1
  155.6 0.0 copy-start
  155.6 1.1 copy.28
  156.7 0.8 copy-done
  157.5 1.1 copy.29
Async XLA Ops:
  145.6 2.4 %copy-start.5 = (bf16[352,2048]{1,0:T(8,128)(2,1)S(1)}, bf16[352,2048]{1,0:T(8,128)(2,1)}, u32[]{:S(2)}) copy-start(bf16[352,2048]{1,0:T(8,128)(2,1)} %get-tuple-element.15) | copy-start | bytes 4325380
  148.1 1.9 %copy-start.4 = (bf16[352,2048]{1,0:T(8,128)(2,1)S(1)}, bf16[352,2048]{1,0:T(8,128)(2,1)}, u32[]{:S(2)}) copy-start(bf16[352,2048]{1,0:T(8,128)(2,1)} %get-tuple-element.16) | copy-start | bytes 4325380
  149.9 1.9 %copy-start.3 = (bf16[352,2048]{1,0:T(8,128)(2,1)S(1)}, bf16[352,2048]{1,0:T(8,128)(2,1)}, u32[]{:S(2)}) copy-start(bf16[352,2048]{1,0:T(8,128)(2,1)} %get-tuple-element.31) | copy-start | bytes 4325380
  151.8 1.9 %copy-start.2 = (bf16[352,2048]{1,0:T(8,128)(2,1)S(1)}, bf16[352,2048]{1,0:T(8,128)(2,1)}, u32[]{:S(2)}) copy-start(bf16[352,2048]{1,0:T(8,128)(2,1)} %get-tuple-element.18) | copy-start | bytes 4325380
  153.7 1.9 %copy-start.1 = (bf16[352,2048]{1,0:T(8,128)(2,1)S(1)}, bf16[352,2048]{1,0:T(8,128)(2,1)}, u32[]{:S(2)}) copy-start(bf16[352,2048]{1,0:T(8,128)(2,1)} %get-tuple-element.19) | copy-start | bytes 4325380
  155.6 1.9 %copy-start = (bf16[352,2048]{1,0:T(8,128)(2,1)S(1)}, bf16[352,2048]{1,0:T(8,128)(2,1)}, u32[]{:S(2)}) copy-start(bf16[352,2048]{1,0:T(8,128)(2,1)} %get-tuple-element.34) | copy-start | bytes 4325380
